TPU v7x, 32 devices: a whole 2x2x4 slice. The times are simulated.
32 devices in a mesh: sp: 16 (over z, y, x), tp: 2 (over core).
Axes of the slice: x: 2, y: 2, z: 4, core: 2. Of those that a mesh axis runs over, the one named last changes fastest.
Arguments:
- residual: bfloat16 [2048, 4096], P('tp', 'sp'), may hold values from -6 to 6
- values: bfloat16 [4096, 4096], P('sp', 'tp'), may hold values from -6 to 6
- gate_input: bfloat16 [4096, 4096], P('sp', 'tp'), may hold values from -6 to 6
- group_keys: bfloat16 [4096, 3072], P('sp', 'tp'), may hold values from -6 to 6
- time_step: float32 [64, 4096], P('tp', 'sp'), may hold values from -8 to 14
- decay_rate: float32 [64], P('tp'), may hold values from 0 to 2
- skip_gain: float32 [64], P('tp'), may hold values from 0.25 to 2
- conv_values: bfloat16 [4, 4096], P(None, 'tp'), may hold values from -3 to 3
- conv_keys: bfloat16 [4, 3072], P(None, 'tp'), may hold values from -3 to 3
- mix_gain: float32 [4096], P('tp'), may hold values from 0.1 to 1.9
- out_weight: bfloat16 [4096, 2048], P('tp'), may hold values from -0.09375 to 0.09375
- norm_gain: float32 [2048], replicated, may hold values from 0.1 to 1.9
- hidden_gate: bfloat16 [2048, 5120], P('sp', 'tp'), may hold values from -0.125 to 0.125
- hidden_up: bfloat16 [2048, 5120], P('sp', 'tp'), may hold values from -0.125 to 0.125
- hidden_conv: bfloat16 [2, 3, 5120], P(None, None, 'tp'), may hold values from -3.5 to 3.5
- hidden_down: bfloat16 [5120, 2048], P('tp', 'sp'), may hold values from -0.078125 to 0.078125
Outputs:
- layer_out: bfloat16 [2048, 4096], P('tp', 'sp')
All inputs are finite; a program needn't handle non-finite values.
Results may differ from a plain program's by a relative error of at most 0.019.
Values may be sent and summed in bfloat16 or wider, within the bound.
A program may use at most 128 MiB of HBM per device.

v0:
```python
import jax
import jax.numpy as jnp
from jax import lax
from jax.sharding import PartitionSpec as P

GROUP_HEADS = 8
HEAD_SIZE = 64
STATE_WIDE = 128
STATE_NARROW = 64
BLOCK = 128
NORM_FLOOR = 0.1
HIGHEST = lax.Precision.HIGHEST


def from_behind(value, axis, steps):
    count = lax.axis_size(axis)
    first, last = (max(0, -steps), min(count, count - steps))
    return lax.ppermute(value, axis, [(source, source + steps) for source in range(first, last)])


def prefix(shard, axis, join, neutral):
    place = lax.axis_index(axis)
    gathered = jax.tree.map(
        lambda a, kind: lax.all_gather(a.astype(kind), axis),
        shard,
        (jnp.bfloat16, jnp.bfloat16, jnp.bfloat16, jnp.bfloat16),
    )
    state = jax.tree.map(lambda a, e: jnp.zeros_like(a) + jnp.asarray(e, a.dtype), shard, neutral)

    def one(lap, state):
        return join(
            state,
            jax.tree.map(
                lambda a, own: lax.dynamic_index_in_dim(a, lap, 0, False).astype(own.dtype),
                gathered,
                shard,
            ),
        )

    return lax.fori_loop(0, place, one, state)


def from_partner_2(shard, axis, stride):
    return lax.ppermute(shard, axis, [(i, i ^ 1 << stride) for i in range(lax.axis_size(axis))])


def tap_sum(joined, weights, row_count):
    summed = weights[0].astype(jnp.float32) * joined[0:row_count]
    for tap_index in range(1, weights.shape[0]):
        summed = (
            summed
            + weights[tap_index].astype(jnp.float32) * joined[tap_index : tap_index + row_count]
        )
    return summed


def block_heads(inputs, in_keys, out_keys, deltas, decay_rates, skip_table, carried):
    length = inputs.shape[0]
    running = jnp.cumsum(-decay_rates * deltas, axis=0)
    weighted = inputs * deltas[..., None]
    scores = jnp.einsum("ign,jgn->gij", out_keys, in_keys, precision=HIGHEST)
    by_head = jnp.transpose(running, (1, 2, 0))
    between = by_head[..., :, None] - by_head[..., None, :]
    lower_mask = jnp.tril(jnp.ones((length, length), dtype=bool))
    decays = jnp.exp(jnp.where(lower_mask, between, -jnp.inf))
    inside = jnp.einsum("ghij,jghp->ighp", scores[:, None] * decays, weighted, precision=HIGHEST)
    carried_part = (
        jnp.einsum("ign,ghpn->ighp", out_keys, carried, precision=HIGHEST)
        * jnp.exp(running)[..., None]
    )
    to_end = jnp.exp(by_head[..., -1:] - by_head)
    fresh_state = jnp.einsum("jgn,ghj,jghp->ghpn", in_keys, to_end, weighted, precision=HIGHEST)
    updated = carried * jnp.exp(by_head[..., -1])[..., None, None] + fresh_state
    return (inside + carried_part + inputs * skip_table[..., None], updated)


def contract_rows(left, right):
    return lax.dot_general(
        left, right, (((0,), (0,)), ((), ())), preferred_element_type=jnp.float32
    )


def combine_states(first_part, second_part):
    return (
        first_part[0] * second_part[0],
        first_part[1] * second_part[0][..., None, None] + second_part[1],
        first_part[2] * second_part[2],
        first_part[3] * second_part[2][..., None, None] + second_part[3],
    )


def hidden_taps(both_pre, edge_cols, taps, row_count):
    joined_hidden = jnp.concatenate([edge_cols, both_pre], axis=2).astype(jnp.float32)
    conv_total = taps[:, 0, :, None].astype(jnp.float32) * joined_hidden[:, :, 0:row_count]
    for tap_index in range(1, taps.shape[1]):
        conv_total = (
            conv_total
            + taps[:, tap_index, :, None].astype(jnp.float32)
            * joined_hidden[:, :, tap_index : tap_index + row_count]
        )
    return (jax.nn.silu(conv_total[0]) * conv_total[1]).astype(jnp.bfloat16)


def local(
    residual,
    values,
    gate_input,
    group_keys,
    time_step,
    decay_rate,
    skip_gain,
    conv_values,
    conv_keys,
    mix_gain,
    out_weight,
    norm_gain,
    hidden_gate,
    hidden_up,
    hidden_conv,
    hidden_down,
):
    row_count = values.shape[0]
    value_cols = values.shape[1]
    tap_count = conv_values.shape[0]
    tail_rows = jnp.concatenate(
        [values[row_count - tap_count + 1 :], group_keys[row_count - tap_count + 1 :]], axis=1
    )
    before_rows = from_behind(tail_rows, "sp", 1)
    joined_values = jnp.concatenate([before_rows[:, :value_cols], values], axis=0).astype(
        jnp.float32
    )
    joined_keys = jnp.concatenate([before_rows[:, value_cols:], group_keys], axis=0).astype(
        jnp.float32
    )
    group_count = group_keys.shape[1] // (2 * STATE_WIDE + 2 * STATE_NARROW)
    inputs = jax.nn.silu(tap_sum(joined_values, conv_values, row_count)).reshape(
        row_count, group_count, GROUP_HEADS, HEAD_SIZE
    )
    key_rows = jax.nn.silu(tap_sum(joined_keys, conv_keys, row_count)).reshape(
        row_count, group_count, -1
    )
    deltas = jax.nn.softplus(time_step).T.reshape(row_count, group_count, GROUP_HEADS)
    rate_table = decay_rate.reshape(group_count, GROUP_HEADS)
    skip_table = skip_gain.reshape(group_count, GROUP_HEADS)
    running = jnp.cumsum(-rate_table * deltas, axis=0)
    half_heads = GROUP_HEADS // 2
    wide_end = 2 * STATE_WIDE

    def run_kind(head_first, head_last, key_first, state_width):
        in_keys = key_rows[..., key_first : key_first + state_width]
        out_keys = key_rows[..., key_first + state_width : key_first + 2 * state_width]
        carried = jnp.zeros(
            (group_count, head_last - head_first, HEAD_SIZE, state_width), jnp.float32
        )
        block_outs = []
        for block_index in range(row_count // BLOCK):
            row_first = block_index * BLOCK
            row_last = row_first + BLOCK
            block_out, carried = block_heads(
                inputs[row_first:row_last, :, head_first:head_last],
                in_keys[row_first:row_last],
                out_keys[row_first:row_last],
                deltas[row_first:row_last, :, head_first:head_last],
                rate_table[:, head_first:head_last],
                skip_table[:, head_first:head_last],
                carried,
            )
            block_outs.append(block_out)
        return (jnp.concatenate(block_outs, axis=0), carried, out_keys)

    wide_local, wide_state, wide_keys = run_kind(0, half_heads, 0, STATE_WIDE)
    narrow_local, narrow_state, narrow_keys = run_kind(
        half_heads, GROUP_HEADS, wide_end, STATE_NARROW
    )
    span_decay = jnp.exp(running[-1])
    start_value = (
        jnp.ones_like(span_decay[:, :half_heads]),
        jnp.zeros_like(wide_state),
        jnp.ones_like(span_decay[:, half_heads:]),
        jnp.zeros_like(narrow_state),
    )
    incoming = prefix(
        (span_decay[:, :half_heads], wide_state, span_decay[:, half_heads:], narrow_state),
        "sp",
        combine_states,
        start_value,
    )
    growth = jnp.exp(running)[..., None]
    wide_out = (
        wide_local
        + jnp.einsum("ign,ghpn->ighp", wide_keys, incoming[1], precision=HIGHEST)
        * growth[:, :, :half_heads]
    )
    narrow_out = (
        narrow_local
        + jnp.einsum("ign,ghpn->ighp", narrow_keys, incoming[3], precision=HIGHEST)
        * growth[:, :, half_heads:]
    )
    mixer_out = jnp.concatenate([wide_out, narrow_out], axis=2).reshape(row_count, value_cols)
    gated_out = mixer_out * jax.nn.silu(gate_input.astype(jnp.float32))
    squares = lax.psum(jnp.sum(gated_out * gated_out, axis=1), "tp")
    inverse_rms = lax.rsqrt(squares / (value_cols * lax.axis_size("tp")) + NORM_FLOOR)
    normed = (gated_out * inverse_rms[:, None] * mix_gain).astype(jnp.bfloat16)
    mixer_sum = lax.psum_scatter(
        lax.dot_general(
            out_weight, normed, (((0,), (1,)), ((), ())), preferred_element_type=jnp.float32
        ).astype(jnp.bfloat16),
        "tp",
        scatter_dimension=0,
        tiled=True,
    ).astype(jnp.float32)
    own_merged = (residual.astype(jnp.float32) + mixer_sum).astype(jnp.bfloat16)
    merged = lax.all_gather(own_merged, "tp", axis=0, tiled=True)
    merged_wide = merged.astype(jnp.float32)
    inverse_norm = lax.rsqrt(jnp.mean(merged_wide * merged_wide, axis=0) + NORM_FLOOR)
    lifted = (merged_wide * inverse_norm[None, :] * norm_gain[:, None]).astype(jnp.bfloat16)
    hidden_cols = hidden_gate.shape[1]
    edge_taps = hidden_conv.shape[1]
    half_cols = hidden_cols // 2
    parity = lax.axis_index("sp") % 2
    first_member = parity == 0
    sp_count = lax.axis_size("sp")
    weight_rows = hidden_gate.shape[0]
    gate_tiles = jnp.tile(
        jnp.stack([hidden_gate[:, :half_cols], hidden_gate[:, half_cols:]]), (sp_count // 2, 1, 1)
    )
    up_tiles = jnp.tile(
        jnp.stack([hidden_up[:, :half_cols], hidden_up[:, half_cols:]]), (sp_count // 2, 1, 1)
    )
    gate_half, up_half = (
        lax.all_to_all(gate_tiles, "sp", split_axis=0, concat_axis=0, tiled=True),
        lax.all_to_all(up_tiles, "sp", split_axis=0, concat_axis=0, tiled=True),
    )
    gate_half = gate_half.reshape(sp_count * weight_rows, half_cols)
    up_half = up_half.reshape(sp_count * weight_rows, half_cols)
    partner_lifted = from_partner_2(lifted, "sp", 0)
    pair_lifted = jnp.where(
        first_member,
        jnp.concatenate([lifted, partner_lifted], axis=1),
        jnp.concatenate([partner_lifted, lifted], axis=1),
    )
    pair_count = 2 * row_count
    pair_pre = jnp.stack(
        [contract_rows(gate_half, pair_lifted), contract_rows(up_half, pair_lifted)]
    ).astype(jnp.bfloat16)
    pair_edge = from_behind(pair_pre[:, :, pair_count - edge_taps + 1 :], "sp", 2)
    half_taps = lax.dynamic_slice_in_dim(hidden_conv, parity * half_cols, half_cols, 2)
    half_hidden = hidden_taps(pair_pre, pair_edge, half_taps, pair_count)
    own_part = lax.dynamic_slice_in_dim(half_hidden, parity * row_count, row_count, 1)
    for_partner = lax.dynamic_slice_in_dim(half_hidden, (1 - parity) * row_count, row_count, 1)
    from_partner = from_partner_2(for_partner, "sp", 0)
    hidden = jnp.where(
        first_member,
        jnp.concatenate([own_part, from_partner], axis=0),
        jnp.concatenate([from_partner, own_part], axis=0),
    )
    down_whole = lax.all_gather(hidden_down, "sp", axis=1, tiled=True)
    hidden_sum = lax.psum_scatter(
        contract_rows(down_whole, hidden).astype(jnp.bfloat16),
        "tp",
        scatter_dimension=0,
        tiled=True,
    ).astype(jnp.float32)
    return (own_merged.astype(jnp.float32) + hidden_sum).astype(jnp.bfloat16)


def solution(mesh):
    in_specs = (
        P("tp", "sp"),
        P("sp", "tp"),
        P("sp", "tp"),
        P("sp", "tp"),
        P("tp", "sp"),
        P("tp"),
        P("tp"),
        P(None, "tp"),
        P(None, "tp"),
        P("tp"),
        P("tp", None),
        P(),
        P("sp", "tp"),
        P("sp", "tp"),
        P(None, None, "tp"),
        P("tp", "sp"),
    )
    out_specs = P("tp", "sp")
    return jax.shard_map(local, mesh=mesh, in_specs=in_specs, out_specs=out_specs, check_vma=False)
```

profile of v0, /device:TPU:0, one launch (start us, length us, event | category | flops | bytes accessed | tf_op | source)
XLA Modules:
  0.0 622.7 jit_solution(8149238865578526616)
XLA Ops:
  8.2 4.9 collective-permute-start
  22.5 2.4 divide_multiply_fusion.1
  30.2 2.5 fusion.43
  33.9 2.8 tile.8
  36.6 6.0 all-to-all-start
  52.9 125.0 %all-gather.4 = bf16[16,4,4]{2,1,0:T(4,128)(2,1)S(1)} all-gather(bf16[1,4,4]{2,1,0:T(4,128)(2,1)S(1)} %get-tuple-element.151), channel_id=2, replica_groups=mesh['sp'=16,'tp'=2] {'sp'}, dimensions={0}, use_global_device_ids=true | all-gather | bytes 544 | tf_op jit(solution)/shard_map/all_gather | solution.py:24
  177.9 77.3 %all-gather.5 = bf16[16,4,4]{2,1,0:T(4,128)(2,1)S(1)} all-gather(bf16[1,4,4]{2,1,0:T(4,128)(2,1)S(1)} %get-tuple-element.150), channel_id=4, replica_groups=mesh['sp'=16,'tp'=2] {'sp'}, dimensions={0}, use_global_device_ids=true | all-gather | bytes 544 | tf_op jit(solution)/shard_map/all_gather | solution.py:24
  262.3 3.0 fusion.38
  265.3 2.9 fusion.32
  268.3 3.0 fusion.34
  279.2 2.5 psum.7
  281.7 7.0 %fusion.6 = bf16[2048,256]{0,1:T(8,128)(2,1)} fusion(bf16[2048,2048]{1,0:T(8,128)(2,1)} %param.28, f32[2048]{0:T(1024)S(1)} %copy-done.19, f32[256]{0:T(256)S(1)} %add_rsqrt_fusion.1, f32[256,2048]{1,0:T(8,128)S(1)} %copy.153, bf16[256,2048]{1,0:T(8,128)(2,1)S(1)} %copy-done.5), kind=kOutput, calls=%fused_computation.24 | convolution fusion | flops 2152726528 | bytes 12592128 | tf_op jit(solution)/shard_map/dot_general | solution.py:205
  290.1 36.7 %reduce-scatter.3.cloned.1.call-done = bf16[1024,256]{0,1:T(8,128)(2,1)} async-done(((bf16[2048,256]{0,1:T(8,128)(2,1)}), bf16[1024,256]{0,1:T(8,128)(2,1)}) %reduce-scatter.3.cloned.1.call-update) | async-done | bytes 524304 | tf_op jit(solution)/shard_map/reduce_scatter | solution.py:204
  329.6 2.8 tile.20
  332.4 6.9 %all-to-all-start.1 = ((bf16[16,128,1280]{2,1,0:T(8,128)(2,1)}), bf16[16,128,1280]{2,1,0:T(8,128)(2,1)}, u32[]{:S(2)}, u32[]{:S(2)}) async-start(bf16[16,128,1280]{2,1,0:T(8,128)(2,1)} %bitcast.260), calls=%async_computation.2 | async-start | bytes 10485760 | tf_op jit(solution)/shard_map/all_to_all | solution.py:232
  344.5 55.0 %collective-permute-done.1 = bf16[2048,256]{0,1:T(8,128)(2,1)S(1)} collective-permute-done((bf16[2048,256]{0,1:T(8,128)(2,1)S(1)}, bf16[2048,256]{0,1:T(8,128)(2,1)S(1)}, u32[]{:S(2)}, u32[]{:S(2)}) %collective-permute-start.1) | collective-permute-done | bytes 1048608 | tf_op jit(solution)/shard_map/ppermute | solution.py:44
  399.5 5.7 fusion.2
  405.2 75.9 %all-to-all-done.1 = bf16[16,128,1280]{2,1,0:T(8,128)(2,1)} async-done(((bf16[16,128,1280]{2,1,0:T(8,128)(2,1)}), bf16[16,128,1280]{2,1,0:T(8,128)(2,1)}, u32[]{:S(2)}, u32[]{:S(2)}) %all-to-all-start.1) | async-done | bytes 5242912 | tf_op jit(solution)/shard_map/all_to_all | solution.py:232
  481.1 6.7 %fusion.3 = bf16[1,1280,512]{1,2,0:T(8,128)(2,1)S(1)} fusion(bf16[2048,1280]{1,0:T(8,128)(2,1)} %bitcast.75, bf16[2048,256]{0,1:T(8,128)(2,1)} %copy-done.18, bf16[2048,256]{0,1:T(8,128)(2,1)} %copy-done.7, pred[]{:T(512)S(6)} %eq.5), kind=kOutput, calls=%fused_computation.12 | convolution fusion | flops 2694447104 | bytes 8650753 | tf_op jit(solution)/shard_map/dot_general | solution.py:78
  487.8 10.7 %collective-permute-start.2 = (bf16[2,1280,2]{1,2,0:T(2,128)(2,1)S(1)}, bf16[2,1280,2]{1,2,0:T(2,128)(2,1)S(1)}, u32[]{:S(2)}, u32[]{:S(2)}) collective-permute-start(bf16[2,1280,2]{1,2,0:T(2,128)(2,1)S(1)} %pad_maximum_fusion.4), channel_id=1, source_target_pairs={{0,4},{2,6},{4,8},{6,10},{8,12},{10,14},{12,16},{14,18},{16,20},{1... | collective-permute-start | bytes 30728 | tf_op jit(solution)/shard_map/ppermute | solution.py:18
  502.8 30.5 %collective-permute-done.3 = bf16[1280,256]{0,1:T(8,128)(2,1)S(1)} collective-permute-done((bf16[1280,256]{0,1:T(8,128)(2,1)S(1)}, bf16[1280,256]{0,1:T(8,128)(2,1)S(1)}, u32[]{:S(2)}, u32[]{:S(2)}) %collective-permute-start.3) | collective-permute-done | bytes 655392 | tf_op jit(solution)/shard_map/ppermute | solution.py:44
  533.3 59.3 %all-gather.13.cloned.1.call-done = bf16[2560,2048]{1,0:T(8,128)(2,1)} async-done(((bf16[2560,128]{1,0:T(8,128)(2,1)}), bf16[2560,2048]{1,0:T(8,128)(2,1)}) %all-gather.13.cloned.1.call-update) | async-done | bytes 10485776 | tf_op jit(solution)/shard_map/all_gather | solution.py:257
  592.6 7.9 %fusion.7 = bf16[2048,256]{0,1:T(8,128)(2,1)} fusion(bf16[2560,2048]{1,0:T(8,128)(2,1)} %all-gather.13.cloned.1.call-done, bf16[1280,256]{0,1:T(8,128)(2,1)S(1)} %collective-permute-done.3, bf16[1280,256]{0,1:T(8,128)(2,1)S(1)} %get-tuple-element.121, pred[]{:T(512)S(6)} %eq.5), kind=kOutput, calls=%fused_computation.25 | convolution fusion | flops 2690777088 | bytes 12845057 | tf_op jit(solution)/shard_map/dot_general | solution.py:78
  600.5 12.9 %reduce-scatter.5.cloned.1.call-done = bf16[1024,256]{0,1:T(8,128)(2,1)} async-done(((bf16[2048,256]{0,1:T(8,128)(2,1)}), bf16[1024,256]{0,1:T(8,128)(2,1)}) %reduce-scatter.5.cloned.1.call-update) | async-done | bytes 524304 | tf_op jit(solution)/shard_map/reduce_scatter | solution.py:258
  (165 shorter events, 58.0 us)
Async XLA Ops:
  6.5 9.2 %copy-start.8 = (bf16[256,1536]{1,0:T(8,128)(2,1)S(1)}, bf16[256,1536]{1,0:T(8,128)(2,1)}, u32[]{:S(2)}) copy-start(bf16[256,1536]{1,0:T(8,128)(2,1)} %param.21) | copy-start | bytes 2359300
  6.5 9.0 %copy-start.13 = (bf16[4,2048]{1,0:T(4,128)(2,1)S(1)}, bf16[4,2048]{1,0:T(4,128)(2,1)}, u32[]{:S(2)}) copy-start(bf16[4,2048]{1,0:T(4,128)(2,1)} %param.25) | copy-start | bytes 49156
  6.5 9.1 %copy-start.14 = (bf16[4,1536]{1,0:T(4,128)(2,1)S(1)}, bf16[4,1536]{1,0:T(4,128)(2,1)}, u32[]{:S(2)}) copy-start(bf16[4,1536]{1,0:T(4,128)(2,1)} %param.26) | copy-start | bytes 36868
  6.5 264.8 %all-gather.17.cloned.1.call-start = ((), (), s32[]{:S(2)}) async-start(), calls=%async_computation.9 | async-start | bytes 4456448 | tf_op jit(solution)/shard_map/all_gather | solution.py:24
  8.2 8.9 %collective-permute-start = (bf16[3,3584]{1,0:T(4,128)(2,1)S(1)}, bf16[3,3584]{1,0:T(4,128)(2,1)S(1)}, u32[]{:S(2)}, u32[]{:S(2)}) collective-permute-start(bf16[3,3584]{1,0:T(4,128)(2,1)S(1)} %pad_maximum_fusion.3), channel_id=1, source_target_pairs={{0,2},{2,4},{4,6},{6,8},{8,10},{10,12},{12,14},{14,16},{16,18},{18... | collective-permute-start | bytes 64520 | tf_op jit(solution)/shard_map/ppermute | solution.py:18
  26.9 244.4 %all-gather.15.cloned.1.call-start = ((), (), s32[]{:S(2)}) async-start(), calls=%async_computation.8 | async-start | bytes 4456448 | tf_op jit(solution)/shard_map/all_gather | solution.py:24
  36.6 292.9 %all-to-all-start = ((bf16[16,128,1280]{2,1,0:T(8,128)(2,1)}), bf16[16,128,1280]{2,1,0:T(8,128)(2,1)}, u32[]{:S(2)}, u32[]{:S(2)}) async-start(bf16[16,128,1280]{2,1,0:T(8,128)(2,1)} %bitcast.259), calls=%async_computation.1 | async-start | bytes 10485760 | tf_op jit(solution)/shard_map/all_to_all | solution.py:231
  42.6 4.9 copy-start.12
  42.6 8.5 %copy-start.17 = (f32[32]{0:T(128)S(1)}, f32[32]{0:T(128)}, u32[]{:S(2)}) copy-start(f32[32]{0:T(128)} %param.24) | copy-start | bytes 388
  42.7 284.1 %reduce-scatter.3.cloned.1.call-start = ((), (), s32[]{:S(2)}) async-start(), calls=%async_computation.4 | async-start | bytes 1572864 | tf_op jit(solution)/shard_map/reduce_scatter | solution.py:204
  46.4 4.8 copy-start.6
  288.7 40.7 %copy-start.9 = (bf16[128,2560]{1,0:T(8,128)(2,1)S(1)}, bf16[128,2560]{1,0:T(8,128)(2,1)}, u32[]{:S(2)}) copy-start(bf16[128,2560]{1,0:T(8,128)(2,1)} %param.31) | copy-start | bytes 1966084
  288.7 50.7 %all-gather.11.cloned.1.call-start = ((), (), s32[]{:S(2)}) async-start(), calls=%async_computation.5 | async-start | bytes 1572864 | tf_op jit(solution)/shard_map/all_gather | solution.py:213
  328.9 263.7 %all-gather.13.cloned.1.call-start = ((), (), s32[]{:S(2)}) async-start(), calls=%async_computation.6 | async-start | bytes 11141120 | tf_op jit(solution)/shard_map/all_gather | solution.py:257
  332.4 8.6 %copy-start.15 = (f32[2048]{0:T(1024)S(1)}, f32[2048]{0:T(1024)}, u32[]{:S(2)}) copy-start(f32[2048]{0:T(1024)} %param.29) | copy-start | bytes 24580
  332.4 148.7 %all-to-all-start.1 = ((bf16[16,128,1280]{2,1,0:T(8,128)(2,1)}), bf16[16,128,1280]{2,1,0:T(8,128)(2,1)}, u32[]{:S(2)}, u32[]{:S(2)}) async-start(bf16[16,128,1280]{2,1,0:T(8,128)(2,1)} %bitcast.260), calls=%async_computation.2 | async-start | bytes 10485760 | tf_op jit(solution)/shard_map/all_to_all | solution.py:232
  339.4 274.0 %reduce-scatter.5.cloned.1.call-start = ((), (), s32[]{:S(2)}) async-start(), calls=%async_computation.7 | async-start | bytes 1572864 | tf_op jit(solution)/shard_map/reduce_scatter | solution.py:258
  342.5 62.7 %copy-start.7 = (bf16[2048,256]{0,1:T(8,128)(2,1)}, bf16[2048,256]{0,1:T(8,128)(2,1)S(1)}, u32[]{:S(2)}) copy-start(bf16[2048,256]{0,1:T(8,128)(2,1)S(1)} %fusion.14) | copy-start | bytes 3145732
  342.5 56.9 %collective-permute-start.1 = (bf16[2048,256]{0,1:T(8,128)(2,1)S(1)}, bf16[2048,256]{0,1:T(8,128)(2,1)S(1)}, u32[]{:S(2)}, u32[]{:S(2)}) collective-permute-start(bf16[2048,256]{0,1:T(8,128)(2,1)S(1)} %fusion.14), channel_id=1, source_target_pairs={{0,2},{2,0},{4,6},{6,4},{8,10},{10,8},{12,14},{14,12},{16,18},{18,... | collective-permute-start | bytes 3145736 | tf_op jit(solution)/shard_map/ppermute | solution.py:44
  399.5 5.8 copy-start.18
  487.8 10.8 %copy-start.16 = (bf16[2,3,2560]{2,0,1:T(2,128)(2,1)S(1)}, bf16[2,3,2560]{2,0,1:T(2,128)(2,1)}, u32[]{:S(2)}) copy-start(bf16[2,3,2560]{2,0,1:T(2,128)(2,1)} %param.32) | copy-start | bytes 92164
  487.8 11.9 %collective-permute-start.2 = (bf16[2,1280,2]{1,2,0:T(2,128)(2,1)S(1)}, bf16[2,1280,2]{1,2,0:T(2,128)(2,1)S(1)}, u32[]{:S(2)}, u32[]{:S(2)}) collective-permute-start(bf16[2,1280,2]{1,2,0:T(2,128)(2,1)S(1)} %pad_maximum_fusion.4), channel_id=1, source_target_pairs={{0,4},{2,6},{4,8},{6,10},{8,12},{10,14},{12,16},{14,18},{16,20},{1... | collective-permute-start | bytes 30728 | tf_op jit(solution)/shard_map/ppermute | solution.py:18
  502.7 30.6 %collective-permute-start.3 = (bf16[1280,256]{0,1:T(8,128)(2,1)S(1)}, bf16[1280,256]{0,1:T(8,128)(2,1)S(1)}, u32[]{:S(2)}, u32[]{:S(2)}) collective-permute-start(bf16[1280,256]{0,1:T(8,128)(2,1)S(1)} %get-tuple-element.122), channel_id=1, source_target_pairs={{0,2},{2,0},{4,6},{6,4},{8,10},{10,8},{12,14},{14,12},{16,18},{18,... | collective-permute-start | bytes 1966088 | tf_op jit(solution)/shard_map/ppermute | solution.py:44
  592.6 20.9 %copy-start.2 = (bf16[1024,256]{0,1:T(8,128)(2,1)S(1)}, bf16[1024,256]{0,1:T(8,128)(2,1)}, u32[]{:S(2)}) copy-start(bf16[1024,256]{0,1:T(8,128)(2,1)} %add_convert_fusion.1) | copy-start | bytes 1572868
  (8 other events, 17.3 us)
Sparse Core Ops, SparseCore 0:
  27.0 157.4 all-gather.16
  187.2 74.3 all-gather.14
  288.8 37.9 reduce-scatter.2
  329.0 10.1 all-gather.10
  341.7 250.7 all-gather.12
  600.6 12.7 reduce-scatter.4
where the time goes:
time: 632 us; the launch traced here: 623 us
  waiting for transfers between devices  272 us (43%)
  blocking collectives  205 us (32%)
  matrix products  52.4 us (8%)
  starting transfers between devices  30.7 us (5%)
  local copies, waits for them, and re-layouts  26.2 us (4%)
  other arithmetic  21.9 us (3%)
  between operations  14.4 us (2%)
    all_gather x2, blocking collectives, prefix(): lax.all_gather(a.astype(kind), axis)  202 us
    ppermute x2, waiting for transfers between devices, from_partner_2(): lax.ppermute(shard, axis, [(i, i ^ 1 << stride) for i in range(lax.axis_s...  85.5 us
    all_to_all x1, waiting for transfers between devices, local(): lax.all_to_all(up_tiles, 'sp', split_axis=0, concat_axis=0, tiled=True)  75.9 us
    all_gather x1, waiting for transfers between devices, local(): down_whole = lax.all_gather(hidden_down, 'sp', axis=1, tiled=True)  59.3 us
    reduce_scatter x1, waiting for transfers between devices, local(): lax.psum_scatter(lax.dot_general(out_weight, normed, (((0,), (1,)), ((),...  36.7 us
    dot_general x3, matrix products, contract_rows(): lax.dot_general(left, right, (((0,), (0,)), ((), ())), preferred_element_...  20.3 us
    ppermute x2, starting transfers between devices, from_behind(): lax.ppermute(value, axis, [(source, source + steps) for source in range(f...  15.6 us
    reduce_scatter x1, waiting for transfers between devices, local(): lax.psum_scatter(contract_rows(down_whole, hidden).astype(jnp.bfloat16),...  12.9 us
  transfers between devices with their start and end apart: 12, of which 7 were waited for; matrix products, arithmetic and copies ran while one was open for 13% of the time, Pallas kernels for 0%

commit v1 on v0

--- a/solution.py
+++ b/solution.py
@@ -10,6 +10,18 @@
 BLOCK = 128
 NORM_FLOOR = 0.1
 HIGHEST = lax.Precision.HIGHEST
+
+
+def collect(value, axis, dim):
+    ways, here = (lax.axis_size(axis), lax.axis_index(axis))
+    grown, reach = (value, 1)
+    while reach < ways:
+        theirs = lax.ppermute(grown, axis, [(d, d ^ reach) for d in range(ways)])
+        mine_first = jnp.concatenate([grown, theirs], axis=dim)
+        theirs_first = jnp.concatenate([theirs, grown], axis=dim)
+        grown = jnp.where(here & reach == 0, mine_first, theirs_first)
+        reach = 2 * reach
+    return grown
 
 
 def from_behind(value, axis, steps):
@@ -254,7 +266,7 @@
         jnp.concatenate([own_part, from_partner], axis=0),
         jnp.concatenate([from_partner, own_part], axis=0),
     )
-    down_whole = lax.all_gather(hidden_down, "sp", axis=1, tiled=True)
+    down_whole = collect(hidden_down, "sp", 1)
     hidden_sum = lax.psum_scatter(
         contract_rows(down_whole, hidden).astype(jnp.bfloat16),
         "tp",

time: 632 us -> 733 us (1.16)
  waiting for transfers between devices: 272 us -> 332 us
  starting transfers between devices: 30.7 us -> 53.1 us
  other arithmetic: 21.9 us -> 35.8 us
    ppermute x0 -> x4, waiting for transfers between devices: none -> 279 us  [collect(): theirs = lax.ppermute(grown, axis, [(d, d ^ reach) for d in range(ways)])]
    ppermute x2, waiting for transfers between devices: 85.5 us -> 0.01 us  [from_partner_2(): lax.ppermute(shard, axis, [(i, i ^ 1 << stride) for i in range(lax.axis_s...]
    all_to_all x1, waiting for transfers between devices: 75.9 us -> 0.01 us  [local(): lax.all_to_all(up_tiles, 'sp', split_axis=0, concat_axis=0, tiled=True)]
    all_gather x1 -> x0, waiting for transfers between devices: 59.3 us -> none  [local(): down_whole = lax.all_gather(hidden_down, 'sp', axis=1, tiled=True)]
    reduce_scatter x1, waiting for transfers between devices: 36.7 us -> 0.02 us  [local(): lax.psum_scatter(lax.dot_general(out_weight, normed, (((0,), (1,)), ((),...]
    ppermute x0 -> x4, starting transfers between devices: none -> 28.5 us  [collect(): theirs = lax.ppermute(grown, axis, [(d, d ^ reach) for d in range(ways)])]
    all_gather x1, waiting for transfers between devices: 0.02 us -> 21 us  [local(): merged = lax.all_gather(own_merged, 'tp', axis=0, tiled=True)]
    reduce_scatter x1, waiting for transfers between devices: 12.9 us -> 30.5 us  [local(): lax.psum_scatter(contract_rows(down_whole, hidden).astype(jnp.bfloat16),...]
  transfers between devices with their start and end apart: 12 -> 15, of which waited for: 7 -> 6; matrix products, arithmetic and copies ran while one was open for 13% -> 13% of each run, Pallas kernels for 0% -> 0%
where the time goes in v1:
time: 733 us; the launch traced here: 723 us
  waiting for transfers between devices  332 us (45%)
  blocking collectives  200 us (27%)
  matrix products  59.4 us (8%)
  starting transfers between devices  53.1 us (7%)
  other arithmetic  35.8 us (5%)
  local copies, waits for them, and re-layouts  28.1 us (4%)
  between operations  14.1 us (2%)
    ppermute x4, waiting for transfers between devices, collect(): theirs = lax.ppermute(grown, axis, [(d, d ^ reach) for d in range(ways)])  279 us
    all_gather x2, blocking collectives, prefix(): lax.all_gather(a.astype(kind), axis)  198 us
    reduce_scatter x1, waiting for transfers between devices, local(): lax.psum_scatter(contract_rows(down_whole, hidden).astype(jnp.bfloat16),...  30.5 us
    ppermute x4, starting transfers between devices, collect(): theirs = lax.ppermute(grown, axis, [(d, d ^ reach) for d in range(ways)])  28.5 us
    dot_general x3, matrix products, contract_rows(): lax.dot_general(left, right, (((0,), (0,)), ((), ())), preferred_element_...  26.6 us
    all_gather x1, waiting for transfers between devices, local(): merged = lax.all_gather(own_merged, 'tp', axis=0, tiled=True)  21 us
  transfers between devices with their start and end apart: 15, of which 6 were waited for; matrix products, arithmetic and copies ran while one was open for 13% of the time, Pallas kernels for 0%

profile of v1, /device:TPU:0, one launch (start us, length us, event | category | flops | bytes accessed | tf_op | source)
XLA Modules:
  0.0 723.2 jit_solution(16124550123569989596)
XLA Ops:
  8.2 4.9 collective-permute-start
  31.8 6.0 all-to-all-start
  55.6 119.0 %all-gather.4 = bf16[16,4,4]{2,1,0:T(4,128)(2,1)S(1)} all-gather(bf16[1,4,4]{2,1,0:T(4,128)(2,1)S(1)} %get-tuple-element.151), channel_id=2, replica_groups=mesh['sp'=16,'tp'=2] {'sp'}, dimensions={0}, use_global_device_ids=true | all-gather | bytes 544 | tf_op jit(solution)/shard_map/all_gather | solution.py:36
  174.6 79.0 %all-gather.5 = bf16[16,4,4]{2,1,0:T(4,128)(2,1)S(1)} all-gather(bf16[1,4,4]{2,1,0:T(4,128)(2,1)S(1)} %get-tuple-element.150), channel_id=4, replica_groups=mesh['sp'=16,'tp'=2] {'sp'}, dimensions={0}, use_global_device_ids=true | all-gather | bytes 544 | tf_op jit(solution)/shard_map/all_gather | solution.py:36
  259.8 3.0 fusion.43
  262.8 3.0 fusion.45
  268.7 3.0 fusion.41
  274.6 4.6 all-to-all-start.1
  290.4 7.0 fusion.14
  299.6 5.7 collective-permute-start.2
  305.3 52.1 %collective-permute-done.2 = bf16[2560,256]{1,0:T(8,128)(2,1)} collective-permute-done((bf16[2560,256]{1,0:T(8,128)(2,1)S(1)}, bf16[2560,256]{1,0:T(8,128)(2,1)}, u32[]{:S(2)}, u32[]{:S(2)}) %collective-permute-start.2) | collective-permute-done | bytes 1310752 | tf_op jit(solution)/shard_map/ppermute | solution.py:19
  357.4 3.0 maximum_select_fusion.3
  360.4 8.8 %collective-permute-start.3 = (bf16[2560,512]{1,0:T(8,128)(2,1)S(1)}, bf16[2560,512]{1,0:T(8,128)(2,1)}, u32[]{:S(2)}, u32[]{:S(2)}) collective-permute-start(bf16[2560,512]{1,0:T(8,128)(2,1)S(1)} %maximum_select_fusion.3), channel_id=1, source_target_pairs={{0,8},{2,10},{4,12},{6,14},{8,0},{10,2},{12,4},{14,6},{16,24},{18,... | collective-permute-start | bytes 7864328 | tf_op jit(solution)/shard_map/ppermute | solution.py:19
  372.8 21.0 %all-gather.10.cloned.1.call-done = bf16[2048,256]{0,1:T(8,128)(2,1)} async-done(((bf16[1024,256]{0,1:T(8,128)(2,1)}), bf16[2048,256]{0,1:T(8,128)(2,1)}) %all-gather.10.cloned.1.call-update) | async-done | bytes 1048592 | tf_op jit(solution)/shard_map/all_gather | solution.py:225
  399.6 26.8 %collective-permute-done.3 = bf16[2560,512]{1,0:T(8,128)(2,1)} collective-permute-done((bf16[2560,512]{1,0:T(8,128)(2,1)S(1)}, bf16[2560,512]{1,0:T(8,128)(2,1)}, u32[]{:S(2)}, u32[]{:S(2)}) %collective-permute-start.3) | collective-permute-done | bytes 2621472 | tf_op jit(solution)/shard_map/ppermute | solution.py:19
  426.4 6.9 maximum_select_fusion.2
  433.3 12.1 %collective-permute-start.4 = (bf16[2560,1024]{1,0:T(8,128)(2,1)}, bf16[2560,1024]{1,0:T(8,128)(2,1)}, u32[]{:S(2)}, u32[]{:S(2)}) collective-permute-start(bf16[2560,1024]{1,0:T(8,128)(2,1)} %maximum_select_fusion.2), channel_id=1, source_target_pairs={{0,16},{2,18},{4,20},{6,22},{8,24},{10,26},{12,28},{14,30},{16,0},... | collective-permute-start | bytes 15728648 | tf_op jit(solution)/shard_map/ppermute | solution.py:19
  445.4 6.7 fusion.9
  452.0 6.8 fusion.10
  458.9 3.8 collective-permute-start.6
  467.1 3.2 collective-permute-start.7
  470.3 200.3 %collective-permute-done.4 = bf16[2560,1024]{1,0:T(8,128)(2,1)} collective-permute-done((bf16[2560,1024]{1,0:T(8,128)(2,1)}, bf16[2560,1024]{1,0:T(8,128)(2,1)}, u32[]{:S(2)}, u32[]{:S(2)}) %collective-permute-start.4) | collective-permute-done | bytes 5242912 | tf_op jit(solution)/shard_map/ppermute | solution.py:19
  670.6 13.2 %fusion.13 = bf16[2048,256]{0,1:T(8,128)(2,1)} fusion(bf16[2560,1024]{1,0:T(8,128)(2,1)} %collective-permute-done.4, bf16[2560,1024]{1,0:T(8,128)(2,1)} %maximum_select_fusion.2, pred[]{:T(512)S(6)} %eq.17, bf16[1280,256]{0,1:T(8,128)(2,1)S(1)} %collective-permute-done.7, bf16[1280,256]{0,1:T(8,128)(2,1)S(1)} %get-tuple-element.121, pred[]{:T(512)S(6)} %eq.21), kind=kOutput, calls=%fused_computation.32 | convolution fusion | flops 2737963008 | bytes 12845058 | tf_op jit(solution)/shard_map/dot_general | solution.py:90
  683.7 30.5 %reduce-scatter.5.cloned.1.call-done = bf16[1024,256]{0,1:T(8,128)(2,1)} async-done(((bf16[2048,256]{0,1:T(8,128)(2,1)}), bf16[1024,256]{0,1:T(8,128)(2,1)}) %reduce-scatter.5.cloned.1.call-update) | async-done | bytes 524304 | tf_op jit(solution)/shard_map/reduce_scatter | solution.py:270
  (169 shorter events, 78.9 us)
Async XLA Ops:
  6.5 10.0 %copy-start.8 = (bf16[256,1536]{1,0:T(8,128)(2,1)S(1)}, bf16[256,1536]{1,0:T(8,128)(2,1)}, u32[]{:S(2)}) copy-start(bf16[256,1536]{1,0:T(8,128)(2,1)} %param.21) | copy-start | bytes 2359300
  6.5 10.0 %copy-start.13 = (bf16[4,1536]{1,0:T(4,128)(2,1)S(1)}, bf16[4,1536]{1,0:T(4,128)(2,1)}, u32[]{:S(2)}) copy-start(bf16[4,1536]{1,0:T(4,128)(2,1)} %param.26) | copy-start | bytes 36868
  6.5 272.7 %all-gather.14.cloned.1.call-start = ((), (), s32[]{:S(2)}) async-start(), calls=%async_computation.8 | async-start | bytes 4456448 | tf_op jit(solution)/shard_map/all_gather | solution.py:36
  8.2 9.8 %collective-permute-start = (bf16[3,3584]{1,0:T(4,128)(2,1)S(1)}, bf16[3,3584]{1,0:T(4,128)(2,1)S(1)}, u32[]{:S(2)}, u32[]{:S(2)}) collective-permute-start(bf16[3,3584]{1,0:T(4,128)(2,1)S(1)} %pad_maximum_fusion.3), channel_id=1, source_target_pairs={{0,2},{2,4},{4,6},{6,8},{8,10},{10,12},{12,14},{14,16},{16,18},{18... | collective-permute-start | bytes 64520 | tf_op jit(solution)/shard_map/ppermute | solution.py:30
  31.8 240.0 %all-to-all-start = ((bf16[16,128,1280]{2,1,0:T(8,128)(2,1)}), bf16[16,128,1280]{2,1,0:T(8,128)(2,1)}, u32[]{:S(2)}, u32[]{:S(2)}) async-start(bf16[16,128,1280]{2,1,0:T(8,128)(2,1)} %bitcast.257), calls=%async_computation.1 | async-start | bytes 10485760 | tf_op jit(solution)/shard_map/all_to_all | solution.py:243
  37.8 241.5 %all-gather.12.cloned.1.call-start = ((), (), s32[]{:S(2)}) async-start(), calls=%async_computation.7 | async-start | bytes 4456448 | tf_op jit(solution)/shard_map/all_gather | solution.py:36
  43.5 6.8 copy-start.12
  43.5 10.4 %copy-start.16 = (f32[32]{0:T(128)S(1)}, f32[32]{0:T(128)}, u32[]{:S(2)}) copy-start(f32[32]{0:T(128)} %param.24) | copy-start | bytes 388
  43.5 253.9 %collective-permute-start.1 = (bf16[2560,128]{1,0:T(8,128)(2,1)}, bf16[2560,128]{1,0:T(8,128)(2,1)}, u32[]{:S(2)}, u32[]{:S(2)}) collective-permute-start(bf16[2560,128]{1,0:T(8,128)(2,1)} %param.33), channel_id=1, source_target_pairs={{0,2},{2,0},{4,6},{6,4},{8,10},{10,8},{12,14},{14,12},{16,18},{18,... | collective-permute-start | bytes 1966088 | tf_op jit(solution)/shard_map/ppermute | solution.py:19
  49.2 4.8 copy-start.7
  274.6 177.4 %all-to-all-start.1 = ((bf16[16,128,1280]{2,1,0:T(8,128)(2,1)}), bf16[16,128,1280]{2,1,0:T(8,128)(2,1)}, u32[]{:S(2)}, u32[]{:S(2)}) async-start(bf16[16,128,1280]{2,1,0:T(8,128)(2,1)} %bitcast.256), calls=%async_computation.2 | async-start | bytes 10485760 | tf_op jit(solution)/shard_map/all_to_all | solution.py:244
  279.2 91.3 %reduce-scatter.3.cloned.1.call-start = ((), (), s32[]{:S(2)}) async-start(), calls=%async_computation.4 | async-start | bytes 1572864 | tf_op jit(solution)/shard_map/reduce_scatter | solution.py:216
  297.4 96.4 %all-gather.10.cloned.1.call-start = ((), (), s32[]{:S(2)}) async-start(), calls=%async_computation.5 | async-start | bytes 1572864 | tf_op jit(solution)/shard_map/all_gather | solution.py:225
  299.6 5.7 copy-start.2
  299.6 57.8 %collective-permute-start.2 = (bf16[2560,256]{1,0:T(8,128)(2,1)S(1)}, bf16[2560,256]{1,0:T(8,128)(2,1)}, u32[]{:S(2)}, u32[]{:S(2)}) collective-permute-start(bf16[2560,256]{1,0:T(8,128)(2,1)S(1)} %maximum_select_fusion.9), channel_id=1, source_target_pairs={{0,4},{2,6},{4,0},{6,2},{8,12},{10,14},{12,8},{14,10},{16,20},{18,... | collective-permute-start | bytes 3932168 | tf_op jit(solution)/shard_map/ppermute | solution.py:19
  360.4 34.9 %copy-start.14 = (f32[2048]{0:T(1024)S(1)}, f32[2048]{0:T(1024)}, u32[]{:S(2)}) copy-start(f32[2048]{0:T(1024)} %param.29) | copy-start | bytes 24580
  360.4 65.9 %collective-permute-start.3 = (bf16[2560,512]{1,0:T(8,128)(2,1)S(1)}, bf16[2560,512]{1,0:T(8,128)(2,1)}, u32[]{:S(2)}, u32[]{:S(2)}) collective-permute-start(bf16[2560,512]{1,0:T(8,128)(2,1)S(1)} %maximum_select_fusion.3), channel_id=1, source_target_pairs={{0,8},{2,10},{4,12},{6,14},{8,0},{10,2},{12,4},{14,6},{16,24},{18,... | collective-permute-start | bytes 7864328 | tf_op jit(solution)/shard_map/ppermute | solution.py:19
  372.6 341.7 %reduce-scatter.5.cloned.1.call-start = ((), (), s32[]{:S(2)}) async-start(), calls=%async_computation.6 | async-start | bytes 1572864 | tf_op jit(solution)/shard_map/reduce_scatter | solution.py:270
  397.8 47.6 %collective-permute-start.5 = (bf16[2048,256]{0,1:T(8,128)(2,1)}, bf16[2048,256]{0,1:T(8,128)(2,1)}, u32[]{:S(2)}, u32[]{:S(2)}) collective-permute-start(bf16[2048,256]{0,1:T(8,128)(2,1)} %fusion.21), channel_id=1, source_target_pairs={{0,2},{2,0},{4,6},{6,4},{8,10},{10,8},{12,14},{14,12},{16,18},{18,... | collective-permute-start | bytes 3145736 | tf_op jit(solution)/shard_map/ppermute | solution.py:56
  433.3 237.2 %collective-permute-start.4 = (bf16[2560,1024]{1,0:T(8,128)(2,1)}, bf16[2560,1024]{1,0:T(8,128)(2,1)}, u32[]{:S(2)}, u32[]{:S(2)}) collective-permute-start(bf16[2560,1024]{1,0:T(8,128)(2,1)} %maximum_select_fusion.2), channel_id=1, source_target_pairs={{0,16},{2,18},{4,20},{6,22},{8,24},{10,26},{12,28},{14,30},{16,0},... | collective-permute-start | bytes 15728648 | tf_op jit(solution)/shard_map/ppermute | solution.py:19
  458.9 3.9 copy-start.15
  458.9 5.2 collective-permute-start.6
  467.1 203.5 %collective-permute-start.7 = (bf16[1280,256]{0,1:T(8,128)(2,1)S(1)}, bf16[1280,256]{0,1:T(8,128)(2,1)S(1)}, u32[]{:S(2)}, u32[]{:S(2)}) collective-permute-start(bf16[1280,256]{0,1:T(8,128)(2,1)S(1)} %get-tuple-element.122), channel_id=1, source_target_pairs={{0,2},{2,0},{4,6},{6,4},{8,10},{10,8},{12,14},{14,12},{16,18},{18,... | collective-permute-start | bytes 1966088 | tf_op jit(solution)/shard_map/ppermute | solution.py:56
  670.6 43.7 %copy-start.3 = (bf16[1024,256]{0,1:T(8,128)(2,1)S(1)}, bf16[1024,256]{0,1:T(8,128)(2,1)}, u32[]{:S(2)}) copy-start(bf16[1024,256]{0,1:T(8,128)(2,1)} %add_convert_fusion.1) | copy-start | bytes 1572868
  (9 other events, 20.7 us)
Sparse Core Ops, SparseCore 0:
  27.9 160.4 all-gather.13
  191.1 81.1 all-gather.11
  297.5 43.0 reduce-scatter.2
  372.7 21.0 all-gather.9
  683.9 30.3 reduce-scatter.4
